TPU v7x, 32 devices: a whole 2x2x4 slice. The times are simulated.
32 devices in a mesh: gr: 2 (over core), fs: 8 (over z, y), tp: 2 (over x).
Axes of the slice: x: 2, y: 2, z: 4, core: 2. Of those that a mesh axis runs over, the one named last changes fastest.
Arguments:
- tokens: bfloat16 [3072, 2048], P(('gr', 'fs')), may hold values from -6 to 6
- routes: int32 [3072, 8], P(('gr', 'fs')), may hold values from 0 to 15, all different within a row; in each aligned block of 192 rows (0 to 191, 192 to 383, ...) at most 144 rows name the same one
- route_weight: float32 [3072, 8], P(('gr', 'fs')), may hold values from 0.05 to 0.6
- norm_gain: float32 [2048], replicated, may hold values from 0.1 to 1.9
- gate_experts: float32 [2, 8, 512, 2048], P('gr', None, 'fs', 'tp'), may hold values from -0.125 to 0.125
- up_experts: float32 [2, 8, 512, 2048], P('gr', None, 'fs', 'tp'), may hold values from -0.125 to 0.125
- down_experts: float32 [2, 8, 512, 2048], P('gr', None, 'fs', 'tp'), may hold values from -0.25 to 0.25
- gate_shared: float32 [2048, 512], P('fs', 'tp'), may hold values from -0.125 to 0.125
- up_shared: float32 [2048, 512], P('fs', 'tp'), may hold values from -0.125 to 0.125
- down_shared: float32 [512, 2048], P('fs', 'tp'), may hold values from -0.25 to 0.25
Outputs:
- mixed: bfloat16 [3072, 2048], P(('gr', 'fs'), 'tp')
- gate_served: bfloat16 [2, 8, 512, 2048], P(None, 'fs', 'tp')
- up_served: bfloat16 [2, 8, 512, 2048], P(None, 'fs', 'tp')
- down_served: bfloat16 [2, 8, 512, 2048], P(None, 'fs', None, 'tp')
- gate_shared_served: bfloat16 [2048, 512], P(None, 'tp')
- up_shared_served: bfloat16 [2048, 512], P(None, 'tp')
- down_shared_served: bfloat16 [512, 2048], P(None, 'tp')
Inputs may be any that keep to these rules, and one draw needn't show every extreme that they name: `routes`: each row names 8 different experts; within the 192 rows of one device no expert is named by more than 144 rows, and some expert reaches 144.
All inputs are finite; a program needn't handle non-finite values.
Results may differ from a plain program's by a relative error of at most 0.0084.
Values may be sent and summed in bfloat16 or wider, within the bound.
A program may use at most 128 MiB of HBM per device.

v0:
```python
import jax
import jax.numpy as jnp
from jax import lax
from jax.sharding import PartitionSpec as P

EXP_HALF = 1
EPS = 1e-06


def on_device(
    tokens,
    routes,
    route_weight,
    norm_gain,
    gate_experts,
    up_experts,
    down_experts,
    gate_shared,
    up_shared,
    down_shared,
):
    bf = jnp.bfloat16
    f32 = jnp.float32
    n_fs = lax.axis_size("fs")
    n_gr = lax.axis_size("gr")
    n_tp = lax.axis_size("tp")
    fs_index = lax.axis_index("fs")
    cols_here = gate_experts.shape[3]
    gain_cols = lax.dynamic_slice_in_dim(norm_gain, lax.axis_index("tp") * cols_here, cols_here, 0)
    gate_local = (gate_experts * gain_cols[None, None, None, :]).astype(bf)
    up_local = (up_experts * gain_cols[None, None, None, :]).astype(bf)
    down_local = down_experts.astype(bf)
    shared_here = gate_shared.shape[0]
    gain_shared = lax.dynamic_slice_in_dim(norm_gain, fs_index * shared_here, shared_here, 0)
    gate_sh_local = (gate_shared * gain_shared[:, None]).astype(bf)
    up_sh_local = (up_shared * gain_shared[:, None]).astype(bf)
    down_sh_local = down_shared.astype(bf)
    halves = (
        lax.all_gather(gate_local, "gr", axis=0, tiled=True),
        lax.all_gather(up_local, "gr", axis=0, tiled=True),
        lax.all_gather(down_local, "gr", axis=0, tiled=True),
    )
    gate_cols, up_cols, down_w = (
        lax.all_to_all(halves[0], "fs", split_axis=1, concat_axis=2, tiled=True),
        lax.all_to_all(halves[1], "fs", split_axis=1, concat_axis=2, tiled=True),
        lax.all_to_all(halves[2], "fs", split_axis=1, concat_axis=2, tiled=True),
    )
    gate_w, up_w = (
        lax.all_to_all(gate_cols, "tp", split_axis=2, concat_axis=3, tiled=True),
        lax.all_to_all(up_cols, "tp", split_axis=2, concat_axis=3, tiled=True),
    )
    gate_sw, up_sw, down_sw = (
        lax.all_gather(gate_sh_local, "fs", axis=0, tiled=True),
        lax.all_gather(up_sh_local, "fs", axis=0, tiled=True),
        lax.all_gather(down_sh_local, "fs", axis=0, tiled=True),
    )
    values = tokens.astype(f32)
    normed = (values * lax.rsqrt(jnp.mean(values * values, axis=-1, keepdims=True) + EPS)).astype(
        bf
    )
    tok_count, top = routes.shape
    width = tokens.shape[1]
    per_group = gate_experts.shape[1]
    count = per_group * n_gr
    capacity = (3 * tok_count * top + 2 * count - 1) // (2 * count)
    flat_e = routes.reshape(-1)
    onehot = (flat_e[:, None] == jnp.arange(count, dtype=jnp.int32)[None, :]).astype(jnp.int32)
    ranks = jnp.sum(jnp.cumsum(onehot, axis=0) * onehot, axis=1) - 1
    group_of = flat_e // per_group
    within = flat_e % per_group
    target = within // EXP_HALF
    local_k = within % EXP_HALF
    slot = ((target * n_gr + group_of) * EXP_HALF + local_k) * capacity + ranks
    total_slots = n_fs * n_gr * EXP_HALF * capacity
    repeated = jnp.repeat(normed, top, axis=0)
    send = jnp.zeros((total_slots, width), bf).at[slot].set(repeated)
    send = send.reshape(n_fs, n_gr, EXP_HALF, capacity, width)
    cols = width // n_tp
    send = lax.dynamic_slice_in_dim(send, lax.axis_index("tp") * cols, cols, 4)
    received = lax.all_to_all(send, "fs", split_axis=0, concat_axis=0, tiled=True)
    received = lax.all_gather(received, "tp", axis=4, tiled=True)
    gate = jnp.einsum("sgkcd,gkfd->sgkcf", received, gate_w, preferred_element_type=f32)
    upper = jnp.einsum("sgkcd,gkfd->sgkcf", received, up_w, preferred_element_type=f32)
    hidden = (jax.nn.silu(gate) * upper).astype(bf)
    full_hidden = lax.all_gather(hidden, "tp", axis=4, tiled=True)
    result = jnp.einsum(
        "sgkcf,gkfe->sgkce", full_hidden, down_w, preferred_element_type=f32
    ).astype(bf)
    returned = lax.all_to_all(result, "fs", split_axis=0, concat_axis=0, tiled=True)
    picked = returned.reshape(total_slots, cols)[slot].reshape(tok_count, top, cols)
    routed = jnp.einsum("tkc,tk->tc", picked.astype(f32), route_weight)
    shared_gate = jnp.dot(normed, gate_sw, preferred_element_type=f32)
    shared_up = jnp.dot(normed, up_sw, preferred_element_type=f32)
    shared_hidden = (jax.nn.silu(shared_gate) * shared_up).astype(bf)
    shared_full = lax.all_gather(shared_hidden, "tp", axis=1, tiled=True)
    shared = jnp.dot(shared_full, down_sw, preferred_element_type=f32)
    mixed = (routed + shared).astype(bf)
    return (mixed, gate_w, up_w, down_w, gate_sw, up_sw, down_sw)


def solution(mesh):
    return jax.shard_map(
        on_device,
        mesh=mesh,
        in_specs=(
            P(("gr", "fs"), None),
            P(("gr", "fs"), None),
            P(("gr", "fs"), None),
            P(),
            P("gr", None, "fs", "tp"),
            P("gr", None, "fs", "tp"),
            P("gr", None, "fs", "tp"),
            P("fs", "tp"),
            P("fs", "tp"),
            P("fs", "tp"),
        ),
        out_specs=(
            P(("gr", "fs"), "tp"),
            P(None, "fs", "tp", None),
            P(None, "fs", "tp", None),
            P(None, "fs", None, "tp"),
            P(None, "tp"),
            P(None, "tp"),
            P(None, "tp"),
        ),
        check_vma=False,
    )
```

profile of v0, /device:TPU:0, one launch (start us, length us, event | category | flops | bytes accessed | tf_op | source)
XLA Modules:
  0.0 651.1 jit_solution(783318843968911715)
XLA Ops:
  8.0 0.9 copy.58
  9.2 4.5 reduce-window.6
  14.6 1.4 fusion.21
  16.2 14.7 %scatter_custom_fusion = bf16[2304,2048]{1,0:T(8,128)(2,1)} fusion(s32[1536]{0:T(1024)S(1)} %fusion.28, bf16[]{:T(256)} %constant.72.clone.1, bf16[192,2048]{1,0:T(8,128)(2,1)S(1)} %fusion.22), kind=kCustom, calls=%fused_computation.6 | custom fusion | bytes 10223618 | tf_op jit(solution)/shard_map/scatter | solution.py:76
  30.9 5.3 dynamic-slice_bitcast_fusion
  36.2 7.4 %all-to-all-start.2 = ((bf16[8,2,1,144,1024]{4,3,1,2,0:T(8,128)(2,1)}), bf16[8,2,1,144,1024]{4,3,1,2,0:T(8,128)(2,1)}, u32[]{:S(2)}, u32[]{:S(2)}) async-start(bf16[8,2,1,144,1024]{4,3,1,2,0:T(8,128)(2,1)} %dynamic-slice_bitcast_fusion), calls=%async_computation.2 | async-start | bytes 9437184 | tf_op jit(solution)/shard_map/all_to_all | solution.py:80
  43.7 3.5 multiply_convert_fusion.1
  47.3 0.7 all-gather.9.cloned.1.call-update
  48.0 0.8 copy-done.6
  48.8 1.1 convert_element_type.57
  49.9 9.4 %all-gather.13.cloned.1.call-done = bf16[2,8,64,1024]{3,2,1,0:T(8,128)(2,1)} async-done(((bf16[1,8,64,1024]{3,2,1,0:T(8,128)(2,1)}), bf16[2,8,64,1024]{3,2,1,0:T(8,128)(2,1)}) %all-gather.13.cloned.1.call-update) | async-done | bytes 2097168 | tf_op jit(solution)/shard_map/all_gather | solution.py:40
  59.3 3.1 copy.63
  62.4 85.7 %all-to-all-done.2 = bf16[8,2,1,144,1024]{4,3,1,2,0:T(8,128)(2,1)} async-done(((bf16[8,2,1,144,1024]{4,3,1,2,0:T(8,128)(2,1)}), bf16[8,2,1,144,1024]{4,3,1,2,0:T(8,128)(2,1)}, u32[]{:S(2)}, u32[]{:S(2)}) %all-to-all-start.2) | async-done | bytes 4718624 | tf_op jit(solution)/shard_map/all_to_all | solution.py:80
  148.2 3.6 all-to-all-start.3
  151.8 0.5 all-gather.11.cloned.1.call-start
  152.3 5.3 copy.62
  157.6 3.1 copy.53
  160.8 39.5 %all-to-all-done.3 = bf16[2,8,64,1024]{3,2,0,1:T(8,128)(2,1)S(1)} async-done(((bf16[2,8,64,1024]{3,2,0,1:T(8,128)(2,1)}), bf16[2,8,64,1024]{3,2,0,1:T(8,128)(2,1)S(1)}, u32[]{:S(2)}, u32[]{:S(2)}) %all-to-all-start.3) | async-done | bytes 2097184 | tf_op jit(solution)/shard_map/all_to_all | solution.py:45
  200.2 4.4 all-to-all-start
  204.8 3.5 copy.65
  208.2 44.2 %all-to-all-done = bf16[2,8,64,1024]{3,2,0,1:T(8,128)(2,1)} async-done(((bf16[2,8,64,1024]{3,2,0,1:T(8,128)(2,1)}), bf16[2,8,64,1024]{3,2,0,1:T(8,128)(2,1)}, u32[]{:S(2)}, u32[]{:S(2)}) %all-to-all-start) | async-done | bytes 2097184 | tf_op jit(solution)/shard_map/all_to_all | solution.py:44
  252.4 3.8 all-to-all-start.4
  256.2 1.8 copy.54
  257.9 3.5 copy.55
  261.4 37.9 %all-to-all-done.4 = bf16[2,1,512,1024]{3,0,1,2:T(2,128)(2,1)S(1)} async-done(((bf16[2,1,512,1024]{3,0,1,2:T(2,128)(2,1)}), bf16[2,1,512,1024]{3,0,1,2:T(2,128)(2,1)S(1)}, u32[]{:S(2)}, u32[]{:S(2)}) %all-to-all-start.4) | async-done | bytes 2097184 | tf_op jit(solution)/shard_map/all_to_all | solution.py:50
  299.3 4.8 all-to-all-start.1
  304.2 3.1 copy.68
  307.3 2.2 copy.66
  309.5 3.5 copy.67
  313.0 4.5 reshape.245
  317.5 11.3 %all-to-all-done.1 = bf16[2,1,512,1024]{3,0,1,2:T(2,128)(2,1)} async-done(((bf16[2,1,512,1024]{3,0,1,2:T(2,128)(2,1)}), bf16[2,1,512,1024]{3,0,1,2:T(2,128)(2,1)}, u32[]{:S(2)}, u32[]{:S(2)}) %all-to-all-start.1) | async-done | bytes 2097184 | tf_op jit(solution)/shard_map/all_to_all | solution.py:49
  328.8 6.1 all-to-all-start.5
  335.1 2.2 copy.56
  337.3 1.3 copy-done
  338.6 3.5 copy.57
  342.1 4.5 reshape.244
  346.6 6.0 fusion
  352.6 1.6 copy-done.14
  354.2 4.1 fusion.10
  358.4 24.0 %all-to-all-done.5 = bf16[2,8,64,1024]{3,2,0,1:T(8,128)(2,1)} async-done(((bf16[2,8,64,1024]{3,2,0,1:T(8,128)(2,1)}), bf16[2,8,64,1024]{3,2,0,1:T(8,128)(2,1)}, u32[]{:S(2)}, u32[]{:S(2)}) %all-to-all-start.5) | async-done | bytes 2097184 | tf_op jit(solution)/shard_map/all_to_all | solution.py:46
  382.4 3.1 copy.69
  385.5 9.5 %all-gather.15.cloned.1.call-done = bf16[8,2,1,144,512]{4,3,0,1,2:T(8,128)(2,1)} async-done(((bf16[8,2,1,144,256]{4,3,0,1,2:T(8,128)(2,1)}), bf16[8,2,1,144,512]{4,3,0,1,2:T(8,128)(2,1)}) %all-gather.15.cloned.1.call-update) | async-done | bytes 2359312 | tf_op jit(solution)/shard_map/all_gather | solution.py:85
  395.0 4.9 convert_bitcast_fusion
  399.9 2.7 copy.70
  402.6 5.7 all-to-all-start.6
  408.5 1.8 multiply_convert_fusion.3
  410.3 0.5 all-gather.21.cloned.1.call-update
  410.9 0.7 convert_element_type.65
  411.8 114.1 %all-gather.19.cloned.1.call-done = bf16[2048,256]{1,0:T(8,128)(2,1)} async-done(((bf16[256,256]{1,0:T(8,128)(2,1)}), bf16[2048,256]{1,0:T(8,128)(2,1)}) %all-gather.19.cloned.1.call-update) | async-done | bytes 1048592 | tf_op jit(solution)/shard_map/all_gather | solution.py:53
  525.8 39.1 %all-gather.21.cloned.1.call-done = bf16[2048,256]{1,0:T(8,128)(2,1)} async-done(((bf16[256,256]{1,0:T(8,128)(2,1)}), bf16[2048,256]{1,0:T(8,128)(2,1)}) %all-gather.21.cloned.1.call-update) | async-done | bytes 1048592 | tf_op jit(solution)/shard_map/all_gather | solution.py:54
  565.0 41.5 %all-gather.23.cloned.1.call-done = bf16[512,1024]{1,0:T(8,128)(2,1)} async-done(((bf16[64,1024]{1,0:T(8,128)(2,1)}), bf16[512,1024]{1,0:T(8,128)(2,1)}) %all-gather.23.cloned.1.call-update) | async-done | bytes 1048592 | tf_op jit(solution)/shard_map/all_gather | solution.py:55
  606.5 1.6 fusion.31
  608.1 1.6 fusion.24
  609.7 5.5 all_gather.34
  615.2 3.9 copy.71
  619.2 2.6 copy.72
  621.7 4.1 copy.74
  625.8 2.4 copy.75
  628.2 10.0 %gather_fusion = bf16[1536,1024]{1,0:T(8,128)(2,1)S(1)} fusion(bf16[2304,1024]{1,0:T(8,128)(2,1)} %bitcast.25, s32[2048]{0:T(1024)S(1)} %pad_clamp_fusion), kind=kCustom, calls=%fused_computation | custom fusion | bytes 6297600 | tf_op jit(solution)/shard_map/gather | solution.py:90
  638.3 1.0 fusion.7
  639.5 1.1 fusion.23
  640.6 1.0 copy.88
  641.6 1.0 copy.89
  642.6 1.0 copy.90
  (62 shorter events, 2.7 us)
Async XLA Ops:
  8.0 8.0 %copy-start.5 = (bf16[192,2048]{1,0:T(8,128)(2,1)S(1)}, bf16[192,2048]{1,0:T(8,128)(2,1)}, u32[]{:S(2)}) copy-start(bf16[192,2048]{1,0:T(8,128)(2,1)} %param.10) | copy-start | bytes 2359300
  36.2 7.5 %copy-start.8 = (f32[1,8,64,1024]{3,2,1,0:T(8,128)S(1)}, f32[1,8,64,1024]{3,2,1,0:T(8,128)}, u32[]{:S(2)}) copy-start(f32[1,8,64,1024]{3,2,1,0:T(8,128)} %param.14) | copy-start | bytes 6291460
  36.2 7.5 %dynamic-slice-start = ((f32[2048]{0:T(1024)}, s32[]{:T(128)}), f32[1024]{0:T(1024)S(1)}, s32[]{:S(2)}) async-start(f32[2048]{0:T(1024)} %param.13, s32[]{:T(128)} %select_n.52), calls=%async_computation.15 | async-start | bytes 8704 | tf_op jit(solution)/shard_map/dynamic_slice | solution.py:29
  36.2 112.0 %all-to-all-start.2 = ((bf16[8,2,1,144,1024]{4,3,1,2,0:T(8,128)(2,1)}), bf16[8,2,1,144,1024]{4,3,1,2,0:T(8,128)(2,1)}, u32[]{:S(2)}, u32[]{:S(2)}) async-start(bf16[8,2,1,144,1024]{4,3,1,2,0:T(8,128)(2,1)} %dynamic-slice_bitcast_fusion), calls=%async_computation.2 | async-start | bytes 9437184 | tf_op jit(solution)/shard_map/all_to_all | solution.py:80
  43.6 15.7 %all-gather.13.cloned.1.call-start = ((), (), s32[]{:S(2)}) async-start(), calls=%async_computation.9 | async-start | bytes 3145728 | tf_op jit(solution)/shard_map/all_gather | solution.py:40
  47.2 1.6 copy-start.6
  47.2 110.4 %all-gather.9.cloned.1.call-start = ((), (), s32[]{:S(2)}) async-start(), calls=%async_computation.7 | async-start | bytes 3145728 | tf_op jit(solution)/shard_map/all_gather | solution.py:39
  48.0 256.2 %all-gather.17.cloned.1.call-start = ((), (), s32[]{:S(2)}) async-start(), calls=%async_computation.11 | async-start | bytes 3145728 | tf_op jit(solution)/shard_map/all_gather | solution.py:41
  148.2 52.1 %all-to-all-start.3 = ((bf16[2,8,64,1024]{3,2,0,1:T(8,128)(2,1)}), bf16[2,8,64,1024]{3,2,0,1:T(8,128)(2,1)S(1)}, u32[]{:S(2)}, u32[]{:S(2)}) async-start(bf16[2,8,64,1024]{3,2,0,1:T(8,128)(2,1)} %copy.63), calls=%async_computation.3 | async-start | bytes 4194304 | tf_op jit(solution)/shard_map/all_to_all | solution.py:45
  151.8 194.8 %all-gather.11.cloned.1.call-start = ((), (), s32[]{:S(2)}) async-start(), calls=%async_computation.8 | async-start | bytes 14155776 | tf_op jit(solution)/shard_map/all_gather | solution.py:81
  200.2 52.2 %all-to-all-start = ((bf16[2,8,64,1024]{3,2,0,1:T(8,128)(2,1)}), bf16[2,8,64,1024]{3,2,0,1:T(8,128)(2,1)}, u32[]{:S(2)}, u32[]{:S(2)}) async-start(bf16[2,8,64,1024]{3,2,0,1:T(8,128)(2,1)} %copy.53), calls=%async_computation | async-start | bytes 4194304 | tf_op jit(solution)/shard_map/all_to_all | solution.py:44
  252.4 46.9 %all-to-all-start.4 = ((bf16[2,1,512,1024]{3,0,1,2:T(2,128)(2,1)}), bf16[2,1,512,1024]{3,0,1,2:T(2,128)(2,1)S(1)}, u32[]{:S(2)}, u32[]{:S(2)}) async-start(bf16[2,1,512,1024]{3,0,1,2:T(2,128)(2,1)} %copy.65), calls=%async_computation.4 | async-start | bytes 4194304 | tf_op jit(solution)/shard_map/all_to_all | solution.py:50
  299.3 4.9 copy-start.1
  299.3 29.5 %all-to-all-start.1 = ((bf16[2,1,512,1024]{3,0,1,2:T(2,128)(2,1)}), bf16[2,1,512,1024]{3,0,1,2:T(2,128)(2,1)}, u32[]{:S(2)}, u32[]{:S(2)}) async-start(bf16[2,1,512,1024]{3,0,1,2:T(2,128)(2,1)} %copy.55), calls=%async_computation.1 | async-start | bytes 4194304 | tf_op jit(solution)/shard_map/all_to_all | solution.py:49
  328.8 53.6 %all-to-all-start.5 = ((bf16[2,8,64,1024]{3,2,0,1:T(8,128)(2,1)}), bf16[2,8,64,1024]{3,2,0,1:T(8,128)(2,1)}, u32[]{:S(2)}, u32[]{:S(2)}) async-start(bf16[2,8,64,1024]{3,2,0,1:T(8,128)(2,1)} %copy.68), calls=%async_computation.5 | async-start | bytes 4194304 | tf_op jit(solution)/shard_map/all_to_all | solution.py:46
  334.9 60.1 %all-gather.15.cloned.1.call-start = ((), (), s32[]{:S(2)}) async-start(), calls=%async_computation.10 | async-start | bytes 3538944 | tf_op jit(solution)/shard_map/all_gather | solution.py:85
  337.3 1.3 copy-start
  346.6 6.0 copy-start.7
  346.6 7.6 %copy-start.14 = (bf16[8,2,1,144,2048]{4,3,0,1,2:T(8,128)(2,1)S(1)}, bf16[8,2,1,144,2048]{4,3,0,1,2:T(8,128)(2,1)}, u32[]{:S(2)}) copy-start(bf16[8,2,1,144,2048]{4,3,0,1,2:T(8,128)(2,1)} %all-gather.11.cloned.1.call-done) | copy-start | bytes 28311556
  402.6 5.7 copy-start.12
  402.6 5.8 copy-start.11
  402.6 8.2 %copy-start.10 = (f32[64,1024]{1,0:T(8,128)S(1)}, f32[64,1024]{1,0:T(8,128)}, u32[]{:S(2)}) copy-start(f32[64,1024]{1,0:T(8,128)} %param.19) | copy-start | bytes 786436
  402.6 8.9 %copy-start.13 = (f32[192,8]{0,1:T(8,128)S(1)}, f32[192,8]{0,1:T(8,128)}, u32[]{:S(2)}) copy-start(f32[192,8]{0,1:T(8,128)} %param.12) | copy-start | bytes 18436
  402.6 225.5 %all-to-all-start.6 = ((bf16[8,2,1,144,1024]{4,3,1,2,0:T(8,128)(2,1)}), bf16[8,2,1,144,1024]{4,3,1,2,0:T(8,128)(2,1)}, u32[]{:S(2)}, u32[]{:S(2)}) async-start(bf16[8,2,1,144,1024]{4,3,1,2,0:T(8,128)(2,1)} %copy.70), calls=%async_computation.6 | async-start | bytes 9437184 | tf_op jit(solution)/shard_map/all_to_all | solution.py:89
  408.3 117.5 %all-gather.19.cloned.1.call-start = ((), (), s32[]{:S(2)}) async-start(), calls=%async_computation.12 | async-start | bytes 1179648 | tf_op jit(solution)/shard_map/all_gather | solution.py:53
  410.2 154.7 %all-gather.21.cloned.1.call-start = ((), (), s32[]{:S(2)}) async-start(), calls=%async_computation.13 | async-start | bytes 1179648 | tf_op jit(solution)/shard_map/all_gather | solution.py:54
  410.8 195.7 %all-gather.23.cloned.1.call-start = ((), (), s32[]{:S(2)}) async-start(), calls=%async_computation.14 | async-start | bytes 1179648 | tf_op jit(solution)/shard_map/all_gather | solution.py:55
  621.7 4.1 copy-start.2
  638.2 1.2 copy-start.3
  638.2 2.4 copy-start.4
  639.5 2.1 copy-start.9
Sparse Core Ops, SparseCore 0:
  47.3 11.9 all-gather.12
  61.4 11.7 all-gather.8
  75.3 11.7 all-gather.16
  157.7 138.2 all-gather.10
  358.5 36.4 all-gather.14
Sparse Core Ops, SparseCore 1:
  411.5 114.3 all-gather.18
  528.4 36.5 all-gather.20
  567.5 38.9 all-gather.22
where the time goes:
time: 660 us; the launch traced here: 651 us
  waiting for transfers between devices  457 us (69%)
  local copies, waits for them, and re-layouts  101 us (15%)
  starting transfers between devices  36.7 us (6%)
  matrix products  20.4 us (3%)
  between operations  16 us (2%)
  other arithmetic  13.6 us (2%)
    all_gather x1, waiting for transfers between devices, on_device(): lax.all_gather(gate_sh_local, 'fs', axis=0, tiled=True)  114 us
    all_to_all x1, waiting for transfers between devices, on_device(): lax.all_to_all(send, 'fs', split_axis=0, concat_axis=0, tiled=True)  85.7 us
    all_to_all x1, waiting for transfers between devices, on_device(): lax.all_to_all(halves[0], 'fs', split_axis=1, concat_axis=2, tiled=True)  44.2 us
    all_gather x1, waiting for transfers between devices, on_device(): lax.all_gather(down_sh_local, 'fs', axis=0, tiled=True)  41.5 us
    all_to_all x1, waiting for transfers between devices, on_device(): lax.all_to_all(halves[1], 'fs', split_axis=1, concat_axis=2, tiled=True)  39.5 us
    all_gather x1, waiting for transfers between devices, on_device(): lax.all_gather(up_sh_local, 'fs', axis=0, tiled=True)  39.1 us
    all_to_all x1, waiting for transfers between devices, on_device(): lax.all_to_all(up_cols, 'tp', split_axis=2, concat_axis=3, tiled=True)  37.9 us
    all_to_all x1, waiting for transfers between devices, on_device(): lax.all_to_all(halves[2], 'fs', split_axis=1, concat_axis=2, tiled=True)  24 us
  transfers between devices with their start and end apart: 15, of which 11 were waited for; matrix products, arithmetic and copies ran while one was open for 12% of the time, Pallas kernels for 0%

commit v1 on v0

--- a/solution.py
+++ b/solution.py
@@ -5,6 +5,14 @@
 
 EXP_HALF = 1
 EPS = 1e-06
+
+
+def balance_views(panel, ax_name):
+    base_arr = lax.axis_size(ax_name)
+    back = jnp.split(panel, base_arr, axis=1)
+    built = jnp.stack(back)
+    earlier = lax.all_to_all(built, ax_name, split_axis=0, concat_axis=0)
+    return jnp.concatenate(earlier, axis=2)
 
 
 def on_device(
@@ -42,7 +50,7 @@
     )
     gate_cols, up_cols, down_w = (
         lax.all_to_all(halves[0], "fs", split_axis=1, concat_axis=2, tiled=True),
-        lax.all_to_all(halves[1], "fs", split_axis=1, concat_axis=2, tiled=True),
+        balance_views(halves[1], "fs"),
         lax.all_to_all(halves[2], "fs", split_axis=1, concat_axis=2, tiled=True),
     )
     gate_w, up_w = (

time: 660 us -> 662 us (level)
    unnamed x37 -> x48, local copies, waits for them, and re-layouts: 14.4 us -> 23.7 us
where the time goes in v1:
time: 662 us; the launch traced here: 652 us
  waiting for transfers between devices  456 us (69%)
  local copies, waits for them, and re-layouts  104 us (16%)
  starting transfers between devices  36.8 us (6%)
  matrix products  20.4 us (3%)
  between operations  16 us (2%)
  other arithmetic  13.6 us (2%)
    all_gather x1, waiting for transfers between devices, on_device(): lax.all_gather(gate_sh_local, 'fs', axis=0, tiled=True)  114 us
    all_to_all x1, waiting for transfers between devices, on_device(): lax.all_to_all(send, 'fs', split_axis=0, concat_axis=0, tiled=True)  79.8 us
    all_to_all x1, waiting for transfers between devices, on_device(): lax.all_to_all(halves[0], 'fs', split_axis=1, concat_axis=2, tiled=True)  43.9 us
    all_to_all x1, waiting for transfers between devices, balance_views(): earlier = lax.all_to_all(built, ax_name, split_axis=0, concat_axis=0)  43.1 us
    all_gather x1, waiting for transfers between devices, on_device(): lax.all_gather(down_sh_local, 'fs', axis=0, tiled=True)  41.5 us
    all_gather x1, waiting for transfers between devices, on_device(): lax.all_gather(up_sh_local, 'fs', axis=0, tiled=True)  39.1 us
    all_to_all x1, waiting for transfers between devices, on_device(): lax.all_to_all(up_cols, 'tp', split_axis=2, concat_axis=3, tiled=True)  37.3 us
    all_to_all x1, waiting for transfers between devices, on_device(): lax.all_to_all(halves[2], 'fs', split_axis=1, concat_axis=2, tiled=True)  24 us
  transfers between devices with their start and end apart: 15, of which 11 were waited for; matrix products, arithmetic and copies ran while one was open for 12% of the time, Pallas kernels for 0%

profile of v1, /device:TPU:0, one launch (start us, length us, event | category | flops | bytes accessed | tf_op | source)
XLA Modules:
  0.0 651.9 jit_solution(541479395586688135)
XLA Ops:
  9.2 4.5 reduce-window.6
  14.6 1.4 fusion.23
  16.2 14.7 %scatter_custom_fusion = bf16[2304,2048]{1,0:T(8,128)(2,1)} fusion(s32[1536]{0:T(1024)S(1)} %fusion.38, bf16[]{:T(256)} %constant.72.clone.1, bf16[192,2048]{1,0:T(8,128)(2,1)S(1)} %fusion.24), kind=kCustom, calls=%fused_computation.6 | custom fusion | bytes 10223618 | tf_op jit(solution)/shard_map/scatter | solution.py:84
  30.9 5.2 dynamic-slice_bitcast_fusion
  36.2 7.4 %all-to-all-start.2 = ((bf16[8,2,1,144,1024]{4,3,1,2,0:T(8,128)(2,1)}), bf16[8,2,1,144,1024]{4,3,1,2,0:T(8,128)(2,1)}, u32[]{:S(2)}, u32[]{:S(2)}) async-start(bf16[8,2,1,144,1024]{4,3,1,2,0:T(8,128)(2,1)} %dynamic-slice_bitcast_fusion), calls=%async_computation.2 | async-start | bytes 9437184 | tf_op jit(solution)/shard_map/all_to_all | solution.py:88
  43.7 3.5 fusion.18
  48.8 1.1 convert_element_type.57
  49.9 9.4 %all-gather.13.cloned.1.call-done = bf16[2,8,64,1024]{3,2,0,1:T(8,128)(2,1)} async-done(((bf16[1,8,64,1024]{3,2,0,1:T(8,128)(2,1)}), bf16[2,8,64,1024]{3,2,0,1:T(8,128)(2,1)}) %all-gather.13.cloned.1.call-update) | async-done | bytes 2097168 | tf_op jit(solution)/shard_map/all_gather | solution.py:48
  59.3 1.0 fusion.34
  60.3 1.0 fusion.33
  61.2 1.0 fusion.32
  62.2 1.0 fusion.31
  63.2 1.0 fusion.30
  64.1 1.0 fusion.29
  65.1 1.0 fusion.28
  66.1 1.0 fusion.27
  67.1 1.3 copy-done.7
  68.4 79.8 %all-to-all-done.2 = bf16[8,2,1,144,1024]{4,3,1,2,0:T(8,128)(2,1)} async-done(((bf16[8,2,1,144,1024]{4,3,1,2,0:T(8,128)(2,1)}), bf16[8,2,1,144,1024]{4,3,1,2,0:T(8,128)(2,1)}, u32[]{:S(2)}, u32[]{:S(2)}) %all-to-all-start.2) | async-done | bytes 4718624 | tf_op jit(solution)/shard_map/all_to_all | solution.py:88
  148.1 3.6 all-to-all-start.3
  151.8 5.2 copy.91
  157.1 43.1 %all-to-all-done.3 = bf16[8,2,1,64,1024]{4,3,1,2,0:T(8,128)(2,1)S(1)} async-done(((bf16[8,2,1,64,1024]{4,3,1,2,0:T(8,128)(2,1)}), bf16[8,2,1,64,1024]{4,3,1,2,0:T(8,128)(2,1)S(1)}, u32[]{:S(2)}, u32[]{:S(2)}) %all-to-all-start.3) | async-done | bytes 2097184 | tf_op jit(solution)/shard_map/all_to_all | solution.py:14
  200.2 4.8 all-to-all-start
  205.2 3.5 copy.94
  208.7 43.9 %all-to-all-done = bf16[2,8,64,1024]{3,2,0,1:T(8,128)(2,1)} async-done(((bf16[2,8,64,1024]{3,2,0,1:T(8,128)(2,1)}), bf16[2,8,64,1024]{3,2,0,1:T(8,128)(2,1)}, u32[]{:S(2)}, u32[]{:S(2)}) %all-to-all-start) | async-done | bytes 2097184 | tf_op jit(solution)/shard_map/all_to_all | solution.py:52
  252.6 3.8 all-to-all-start.4
  256.4 5.1 copy.84
  261.5 37.3 %all-to-all-done.4 = bf16[2,1,512,1024]{3,0,1,2:T(2,128)(2,1)S(1)} async-done(((bf16[2,1,512,1024]{3,0,1,2:T(2,128)(2,1)}), bf16[2,1,512,1024]{3,0,1,2:T(2,128)(2,1)S(1)}, u32[]{:S(2)}, u32[]{:S(2)}) %all-to-all-start.4) | async-done | bytes 2097184 | tf_op jit(solution)/shard_map/all_to_all | solution.py:58
  298.8 1.3 copy-done.1
  300.1 4.8 all-to-all-start.1
  305.0 3.3 copy.97
  308.9 3.5 copy.96
  312.4 4.5 reshape.250
  316.9 12.7 %all-to-all-done.1 = bf16[2,1,512,1024]{3,0,1,2:T(2,128)(2,1)} async-done(((bf16[2,1,512,1024]{3,0,1,2:T(2,128)(2,1)}), bf16[2,1,512,1024]{3,0,1,2:T(2,128)(2,1)}, u32[]{:S(2)}, u32[]{:S(2)}) %all-to-all-start.1) | async-done | bytes 2097184 | tf_op jit(solution)/shard_map/all_to_all | solution.py:57
  329.5 6.2 all-to-all-start.5
  335.9 2.2 copy.85
  338.1 1.3 copy-done
  339.4 3.5 copy.86
  342.9 4.5 reshape.249
  347.4 6.0 fusion
  353.4 1.6 copy-done.16
  355.0 4.1 fusion.10
  359.2 24.0 %all-to-all-done.5 = bf16[2,8,64,1024]{3,2,0,1:T(8,128)(2,1)} async-done(((bf16[2,8,64,1024]{3,2,0,1:T(8,128)(2,1)}), bf16[2,8,64,1024]{3,2,0,1:T(8,128)(2,1)}, u32[]{:S(2)}, u32[]{:S(2)}) %all-to-all-start.5) | async-done | bytes 2097184 | tf_op jit(solution)/shard_map/all_to_all | solution.py:54
  383.2 3.1 copy.98
  386.3 9.4 %all-gather.15.cloned.1.call-done = bf16[8,2,1,144,512]{4,3,0,1,2:T(8,128)(2,1)} async-done(((bf16[8,2,1,144,256]{4,3,0,1,2:T(8,128)(2,1)}), bf16[8,2,1,144,512]{4,3,0,1,2:T(8,128)(2,1)}) %all-gather.15.cloned.1.call-update) | async-done | bytes 2359312 | tf_op jit(solution)/shard_map/all_gather | solution.py:93
  395.8 4.9 convert_bitcast_fusion
  400.7 2.7 copy.99
  403.4 5.7 all-to-all-start.6
  409.2 1.8 multiply_convert_fusion.1
  412.5 114.1 %all-gather.19.cloned.1.call-done = bf16[2048,256]{1,0:T(8,128)(2,1)} async-done(((bf16[256,256]{1,0:T(8,128)(2,1)}), bf16[2048,256]{1,0:T(8,128)(2,1)}) %all-gather.19.cloned.1.call-update) | async-done | bytes 1048592 | tf_op jit(solution)/shard_map/all_gather | solution.py:61
  526.6 39.1 %all-gather.21.cloned.1.call-done = bf16[2048,256]{1,0:T(8,128)(2,1)} async-done(((bf16[256,256]{1,0:T(8,128)(2,1)}), bf16[2048,256]{1,0:T(8,128)(2,1)}) %all-gather.21.cloned.1.call-update) | async-done | bytes 1048592 | tf_op jit(solution)/shard_map/all_gather | solution.py:62
  565.8 41.5 %all-gather.23.cloned.1.call-done = bf16[512,1024]{1,0:T(8,128)(2,1)} async-done(((bf16[64,1024]{1,0:T(8,128)(2,1)}), bf16[512,1024]{1,0:T(8,128)(2,1)}) %all-gather.23.cloned.1.call-update) | async-done | bytes 1048592 | tf_op jit(solution)/shard_map/all_gather | solution.py:63
  607.3 1.6 fusion.41
  608.9 1.6 fusion.26
  610.5 5.5 all_gather.34
  616.0 2.5 copy.101
  618.5 4.1 copy.100
  622.6 2.4 copy.104
  625.0 3.9 copy.103
  628.9 10.0 %gather_fusion = bf16[1536,1024]{1,0:T(8,128)(2,1)S(1)} fusion(bf16[2304,1024]{1,0:T(8,128)(2,1)} %bitcast.36, s32[2048]{0:T(1024)S(1)} %pad_clamp_fusion), kind=kCustom, calls=%fused_computation | custom fusion | bytes 6297600 | tf_op jit(solution)/shard_map/gather | solution.py:98
  639.0 1.0 fusion.7
  640.2 1.1 fusion.25
  641.4 1.0 copy.124
  642.4 1.0 copy.125
  643.4 1.0 copy.126
  (71 shorter events, 6.9 us)
Async XLA Ops:
  8.0 8.0 %copy-start.6 = (bf16[192,2048]{1,0:T(8,128)(2,1)S(1)}, bf16[192,2048]{1,0:T(8,128)(2,1)}, u32[]{:S(2)}) copy-start(bf16[192,2048]{1,0:T(8,128)(2,1)} %param.10) | copy-start | bytes 2359300
  36.2 7.5 %copy-start.10 = (f32[1,8,64,1024]{3,2,1,0:T(8,128)S(1)}, f32[1,8,64,1024]{3,2,1,0:T(8,128)}, u32[]{:S(2)}) copy-start(f32[1,8,64,1024]{3,2,1,0:T(8,128)} %param.14) | copy-start | bytes 6291460
  36.2 7.5 %dynamic-slice-start = ((f32[2048]{0:T(1024)}, s32[]{:T(128)}), f32[1024]{0:T(1024)S(1)}, s32[]{:S(2)}) async-start(f32[2048]{0:T(1024)} %param.13, s32[]{:T(128)} %select_n.52), calls=%async_computation.15 | async-start | bytes 8704 | tf_op jit(solution)/shard_map/dynamic_slice | solution.py:37
  36.2 112.0 %all-to-all-start.2 = ((bf16[8,2,1,144,1024]{4,3,1,2,0:T(8,128)(2,1)}), bf16[8,2,1,144,1024]{4,3,1,2,0:T(8,128)(2,1)}, u32[]{:S(2)}, u32[]{:S(2)}) async-start(bf16[8,2,1,144,1024]{4,3,1,2,0:T(8,128)(2,1)} %dynamic-slice_bitcast_fusion), calls=%async_computation.2 | async-start | bytes 9437184 | tf_op jit(solution)/shard_map/all_to_all | solution.py:88
  43.6 15.7 %all-gather.13.cloned.1.call-start = ((), (), s32[]{:S(2)}) async-start(), calls=%async_computation.9 | async-start | bytes 3145728 | tf_op jit(solution)/shard_map/all_gather | solution.py:48
  47.2 1.6 copy-start.8
  47.2 109.9 %all-gather.9.cloned.1.call-start = ((), (), s32[]{:S(2)}) async-start(), calls=%async_computation.7 | async-start | bytes 3145728 | tf_op jit(solution)/shard_map/all_gather | solution.py:47
  47.9 257.0 %all-gather.17.cloned.1.call-start = ((), (), s32[]{:S(2)}) async-start(), calls=%async_computation.11 | async-start | bytes 3145728 | tf_op jit(solution)/shard_map/all_gather | solution.py:49
  67.1 1.3 copy-start.7
  148.1 52.1 %all-to-all-start.3 = ((bf16[8,2,1,64,1024]{4,3,1,2,0:T(8,128)(2,1)}), bf16[8,2,1,64,1024]{4,3,1,2,0:T(8,128)(2,1)S(1)}, u32[]{:S(2)}, u32[]{:S(2)}) async-start(bf16[8,2,1,64,1024]{4,3,1,2,0:T(8,128)(2,1)} %copy-done.7), calls=%async_computation.3 | async-start | bytes 4194304 | tf_op jit(solution)/shard_map/all_to_all | solution.py:14
  151.8 195.6 %all-gather.11.cloned.1.call-start = ((), (), s32[]{:S(2)}) async-start(), calls=%async_computation.8 | async-start | bytes 14155776 | tf_op jit(solution)/shard_map/all_gather | solution.py:89
  200.2 52.4 %all-to-all-start = ((bf16[2,8,64,1024]{3,2,0,1:T(8,128)(2,1)}), bf16[2,8,64,1024]{3,2,0,1:T(8,128)(2,1)}, u32[]{:S(2)}, u32[]{:S(2)}) async-start(bf16[2,8,64,1024]{3,2,0,1:T(8,128)(2,1)} %all-gather.9.cloned.1.call-done), calls=%async_computation | async-start | bytes 4194304 | tf_op jit(solution)/shard_map/all_to_all | solution.py:52
  252.6 46.2 %all-to-all-start.4 = ((bf16[2,1,512,1024]{3,0,1,2:T(2,128)(2,1)}), bf16[2,1,512,1024]{3,0,1,2:T(2,128)(2,1)S(1)}, u32[]{:S(2)}, u32[]{:S(2)}) async-start(bf16[2,1,512,1024]{3,0,1,2:T(2,128)(2,1)} %copy.94), calls=%async_computation.4 | async-start | bytes 4194304 | tf_op jit(solution)/shard_map/all_to_all | solution.py:58
  298.8 1.3 copy-start.1
  300.1 29.4 %all-to-all-start.1 = ((bf16[2,1,512,1024]{3,0,1,2:T(2,128)(2,1)}), bf16[2,1,512,1024]{3,0,1,2:T(2,128)(2,1)}, u32[]{:S(2)}, u32[]{:S(2)}) async-start(bf16[2,1,512,1024]{3,0,1,2:T(2,128)(2,1)} %bitcast.149), calls=%async_computation.1 | async-start | bytes 4194304 | tf_op jit(solution)/shard_map/all_to_all | solution.py:57
  305.0 3.3 copy-start.2
  329.5 53.6 %all-to-all-start.5 = ((bf16[2,8,64,1024]{3,2,0,1:T(8,128)(2,1)}), bf16[2,8,64,1024]{3,2,0,1:T(8,128)(2,1)}, u32[]{:S(2)}, u32[]{:S(2)}) async-start(bf16[2,8,64,1024]{3,2,0,1:T(8,128)(2,1)} %copy.97), calls=%async_computation.5 | async-start | bytes 4194304 | tf_op jit(solution)/shard_map/all_to_all | solution.py:54
  335.7 60.1 %all-gather.15.cloned.1.call-start = ((), (), s32[]{:S(2)}) async-start(), calls=%async_computation.10 | async-start | bytes 3538944 | tf_op jit(solution)/shard_map/all_gather | solution.py:93
  338.1 1.3 copy-start
  347.4 6.0 copy-start.9
  347.4 7.6 %copy-start.16 = (bf16[8,2,1,144,2048]{4,3,0,1,2:T(8,128)(2,1)S(1)}, bf16[8,2,1,144,2048]{4,3,0,1,2:T(8,128)(2,1)}, u32[]{:S(2)}) copy-start(bf16[8,2,1,144,2048]{4,3,0,1,2:T(8,128)(2,1)} %all-gather.11.cloned.1.call-done) | copy-start | bytes 28311556
  403.4 5.7 copy-start.14
  403.4 5.8 copy-start.13
  403.4 8.2 %copy-start.12 = (f32[64,1024]{1,0:T(8,128)S(1)}, f32[64,1024]{1,0:T(8,128)}, u32[]{:S(2)}) copy-start(f32[64,1024]{1,0:T(8,128)} %param.19) | copy-start | bytes 786436
  403.4 8.9 %copy-start.15 = (f32[192,8]{0,1:T(8,128)S(1)}, f32[192,8]{0,1:T(8,128)}, u32[]{:S(2)}) copy-start(f32[192,8]{0,1:T(8,128)} %param.12) | copy-start | bytes 18436
  403.4 225.5 %all-to-all-start.6 = ((bf16[8,2,1,144,1024]{4,3,1,2,0:T(8,128)(2,1)}), bf16[8,2,1,144,1024]{4,3,1,2,0:T(8,128)(2,1)}, u32[]{:S(2)}, u32[]{:S(2)}) async-start(bf16[8,2,1,144,1024]{4,3,1,2,0:T(8,128)(2,1)} %copy.99), calls=%async_computation.6 | async-start | bytes 9437184 | tf_op jit(solution)/shard_map/all_to_all | solution.py:97
  409.1 117.5 %all-gather.19.cloned.1.call-start = ((), (), s32[]{:S(2)}) async-start(), calls=%async_computation.12 | async-start | bytes 1179648 | tf_op jit(solution)/shard_map/all_gather | solution.py:61
  411.0 154.7 %all-gather.21.cloned.1.call-start = ((), (), s32[]{:S(2)}) async-start(), calls=%async_computation.13 | async-start | bytes 1179648 | tf_op jit(solution)/shard_map/all_gather | solution.py:62
  411.6 195.7 %all-gather.23.cloned.1.call-start = ((), (), s32[]{:S(2)}) async-start(), calls=%async_computation.14 | async-start | bytes 1179648 | tf_op jit(solution)/shard_map/all_gather | solution.py:63
  618.5 4.1 copy-start.3
  639.0 1.2 copy-start.4
  640.2 1.2 copy-start.5
  640.2 2.2 copy-start.11
Sparse Core Ops, SparseCore 0:
  47.3 11.9 all-gather.12
  61.4 11.7 all-gather.8
  75.3 11.7 all-gather.16
  157.2 137.6 all-gather.10
  359.3 36.4 all-gather.14
Sparse Core Ops, SparseCore 1:
  412.3 114.3 all-gather.18
  529.2 36.5 all-gather.20
  568.3 38.9 all-gather.22
